TPU v7x, 512 devices: a 8x2x16 block of a 8x8x16 slice. The times are simulated.
512 devices in a mesh: grp: 2 (over y), sp: 16 (over z), tp: 16 (over x, core).
Axes of the slice: x: 8, y: 2, z: 16, core: 2. Of those that a mesh axis runs over, the one named last changes fastest.
The devices are a block of a 8x8x16 slice.
Arguments:
- hidden_items: bfloat16 [4096, 4096], P(('grp', 'sp', 'tp')), parts along dimension 0, may hold values from -6 to 6
- sample_cond: bfloat16 [8192], P('grp'), parts along dimension 0, may hold values from -6 to 6
- prompt_items: bfloat16 [256, 4096], P(('grp', 'sp')), parts along dimension 0, may hold values from -6 to 6
- prompt_cond: bfloat16 [4096], replicated, may hold values from -6 to 6
- adjust_shifting: bfloat16 [4096, 4096], P('sp', 'tp'), may hold values from -0.125 to 0.125
- adjust_stretch: bfloat16 [4096, 4096], P('sp', 'tp'), may hold values from -0.125 to 0.125
- skip_valve: bfloat16 [4096, 4096], P('sp', 'tp'), may hold values from -0.125 to 0.125
- receiver_matrix: bfloat16 [4096, 2048], P(None, 'tp'), may hold values from -0.09375 to 0.09375
- address_matrix: bfloat16 [4096, 2048], P(None, 'tp'), may hold values from -0.09375 to 0.09375
- payload_matrix: bfloat16 [4096, 2048], P(None, 'tp'), may hold values from -0.09375 to 0.09375
- joint_lower_projector: bfloat16 [4096, 64], P('sp'), may hold values from -0.09375 to 0.09375
- fading_raise_matrix: bfloat16 [64, 2048], P(None, 'tp'), may hold values from -1.5 to 1.5
- step_raise_matrix: bfloat16 [64, 2048], P(None, 'tp'), may hold values from -1.5 to 1.5
- feature_fading: float32 [2048], P('tp'), may hold values from 0 to 0.1, as said below
- spike_logfade: float32 [4096, 32], P(('grp', 'sp'), 'tp'), parts along dimension 0, may hold values from 0 to 2
- group_standard_factor: float32 [2048], P('tp'), may hold values from 0.1 to 1.9
- emit_matrix: bfloat16 [2048, 4096], P('tp', 'sp'), may hold values from -0.125 to 0.125
Outputs:
- latent_out: bfloat16 [4096, 4096], P(('grp', 'sp', 'tp')), parts along dimension 0
There are 2 independent parts, one for each index of `grp`. A program takes and returns all parts, laid end to end along the dimension named above; an argument that names none is the same for every part. Nothing has to cross between parts.
Inputs may be any that keep to these rules, and one draw needn't show every extreme that they name: `feature_fading`: per-token decay rate of each channel.
All inputs are finite; a program needn't handle non-finite values.
Results may differ from a plain program's by a relative error of at most 0.015.
Values may be sent and summed in bfloat16 or wider, within the bound.
No kernel may reach another device: no remote copies, remote signals or barrier semaphores. Data moves between devices by JAX's collectives and lax.ppermute only.
A program may use at most 64 MiB of HBM per device.

v0:
```python
import math
import jax
import jax.numpy as jnp
from jax import lax
from jax.sharding import PartitionSpec as P

ATTEND_WIDTH = 64
EPS_ROW = 1e-05
EPS_HEAD = 0.00064
EPS_KEY = 1e-06
rate_shift = 5.0


def copy_for_each(shard, axis):
    peers = lax.axis_size(axis)
    return lax.all_to_all(
        jnp.broadcast_to(shard[None], (peers, *shard.shape)), axis, 0, 0, tiled=True
    )


def of_everyone(shard, axis):
    return copy_for_each(shard, axis).sum(axis=0)


def packed_total(arrays, axis):
    vector, at, gathered = (jnp.concatenate([a.reshape(-1) for a in arrays]), 0, [])
    subtotal = of_everyone(vector, axis)
    for a in arrays:
        gathered.append(subtotal[at : at + a.size].reshape(a.shape))
        at += a.size
    return tuple(gathered)


def in_one_piece(arrays, axis, dim, along):
    ends, at = ([], 0)
    for a in arrays[:-1]:
        at += a.shape[along]
        ends.append(at)
    both = jnp.concatenate(arrays, axis=along)
    return tuple(jnp.split(lax.all_gather(both, axis, axis=dim, tiled=True), ends, axis=along))


def rows_first(arrays, axis, dims):
    turned = [jnp.moveaxis(a, dim, 0) for a, dim in zip(arrays, dims)]
    both = jnp.concatenate([t.reshape(len(t), -1) for t in turned], axis=1)
    result, at, gathered = (lax.all_gather(both, axis, axis=0, tiled=True), 0, [])
    for t, dim in zip(turned, dims):
        slab = result[:, at : at + t[0].size].reshape(-1, *t.shape[1:])
        gathered.append(jnp.moveaxis(slab, 0, dim))
        at += t[0].size
    return tuple(gathered)


def collected_together(shard, axis):
    leaves = jax.tree.leaves(shard)
    order = sorted(range(len(leaves)), key=lambda k: -leaves[k].size)
    width = (1, *leaves[order[0]].shape)[-1]
    lines = [
        jnp.pad(leaves[k].reshape(-1), (0, -leaves[k].size % width)).reshape(-1, width)
        for k in order
    ]
    both, at, found = (lax.all_gather(jnp.concatenate(lines), axis), 0, {})
    for k, line in zip(order, lines):
        slab = both[:, at : at + len(line)].reshape(len(both), -1)
        found[k] = slab[:, : leaves[k].size].reshape(-1, *leaves[k].shape)
        at += len(line)
    numbers = iter(range(len(leaves)))
    return jax.tree.map(lambda _: found[next(numbers)], shard)


def entering(shard, axis, combine, identity):
    peers, mine = (lax.axis_size(axis), lax.axis_index(axis))
    everything = collected_together(
        jax.tree.map(lambda part, kind: part.astype(kind), shard, (jnp.bfloat16, jnp.bfloat16)),
        axis,
    )
    start = jax.tree.map(
        lambda part, zero: jnp.broadcast_to(jnp.asarray(zero, part.dtype), part.shape),
        shard,
        identity,
    )

    def step(k, before):
        reached = k < mine
        new = combine(
            before, jax.tree.map(lambda part, own: part[k].astype(own.dtype), everything, shard)
        )
        return jax.tree.map(lambda a, b: jnp.where(reached, a, b), new, before)

    return lax.fori_loop(0, peers, step, start)


def gathered_once(shard, axis):
    leaves = jax.tree.leaves(shard)
    order = sorted(range(len(leaves)), key=lambda k: -leaves[k].size)
    width = (1, *leaves[order[0]].shape)[-1]
    lines = [
        jnp.pad(leaves[k].reshape(-1), (0, -leaves[k].size % width)).reshape(-1, width)
        for k in order
    ]
    both, at, found = (copy_for_each(jnp.concatenate(lines), axis), 0, {})
    for k, line in zip(order, lines):
        slab = both[:, at : at + len(line)].reshape(len(both), -1)
        found[k] = slab[:, : leaves[k].size].reshape(-1, *leaves[k].shape)
        at += len(line)
    numbers = iter(range(len(leaves)))
    return jax.tree.map(lambda _: found[next(numbers)], shard)


def folded_in_pairs(pieces, combine):
    while len(jax.tree.leaves(pieces)[0]) > 1:
        pieces = jax.vmap(combine)(
            *(jax.tree.map(lambda part: part[side::2], pieces) for side in (0, 1))
        )
    return jax.tree.map(lambda part: part[0], pieces)


def entering_2(shard, axis, combine, identity):
    peers, mine = (lax.axis_size(axis), lax.axis_index(axis))
    passed = jnp.arange(peers) > mine

    def kept(part, zero, own):
        part = jnp.where(
            passed.reshape(-1, *(1 for _ in own.shape)),
            part.astype(own.dtype),
            jnp.asarray(zero, own.dtype),
        )
        return part[::-1]

    pieces = gathered_once(
        jax.tree.map(lambda part, kind: part.astype(kind), shard, (jnp.bfloat16, jnp.bfloat16)),
        axis,
    )
    return folded_in_pairs(jax.tree.map(kept, pieces, identity, shard), combine)


def cut_along(shard, dim, peers):
    dims = shard.shape
    tiles = shard.reshape(*dims[:dim], peers, dims[dim] // peers, *dims[dim + 1 :])
    return jnp.moveaxis(tiles, dim, 0)


def sent_and_summed(shard, axis, dim):
    peers = lax.axis_size(axis)
    tiles = lax.all_to_all(cut_along(shard, dim, peers), axis, 0, 0, tiled=True)
    return jnp.sum(tiles.astype(jnp.float32), axis=0)


def stored(value):
    return lax.optimization_barrier(value.astype(jnp.bfloat16))


def product(left, right):
    return jnp.dot(left, right, preferred_element_type=jnp.float32)


def batch_dot(left, right):
    return jnp.matmul(left, right)


def flipped(tensor):
    return jnp.swapaxes(tensor, -1, -2)


def modulate(rows, shifts, scales):
    values = rows.astype(jnp.float32)
    centre = jnp.mean(values, -1, keepdims=True)
    spread = jnp.mean(jnp.square(values - centre), -1, keepdims=True)
    normed = (values - centre) * lax.rsqrt(spread + EPS_ROW)
    return (normed * (1.0 + scales) + shifts).astype(jnp.bfloat16)


def both_ways(tensor):
    return jnp.stack([tensor, jnp.flip(tensor, axis=1)])


def chain_inputs(
    key_rows,
    value_rows,
    low_rows,
    query_rows,
    fading_raise_matrix,
    step_raise_matrix,
    feature_fading,
    surplus_entries,
):
    row_count = key_rows.shape[0]
    head_count = key_rows.shape[1] // ATTEND_WIDTH
    squashed = jnp.tanh(low_rows.astype(jnp.float32)).astype(jnp.bfloat16)
    logdecay = (
        -feature_fading * jax.nn.sigmoid(product(squashed, fading_raise_matrix)) - surplus_entries
    )
    learned = jax.nn.sigmoid(product(squashed, step_raise_matrix) - rate_shift)

    def by_head(tensor):
        return jnp.transpose(
            tensor.astype(jnp.float32).reshape(row_count, head_count, ATTEND_WIDTH), (1, 0, 2)
        )

    key_heads = by_head(key_rows)
    unit_keys = key_heads * lax.rsqrt(jnp.sum(key_heads * key_heads, -1, keepdims=True) + EPS_KEY)
    removal = unit_keys * by_head(learned)
    return tuple(
        (
            both_ways(tensor)
            for tensor in (
                by_head(logdecay),
                key_heads,
                by_head(value_rows),
                unit_keys,
                removal,
                by_head(query_rows),
            )
        )
    )


def sub_block(carried, inputs, reading):
    logdecay, key_heads, value_heads, unit_keys, removal, query_heads = inputs
    sub_len = logdecay.shape[-2]
    totals = jnp.cumsum(logdecay, axis=-2)
    inclusive = jnp.exp(totals)
    exclusive = jnp.exp(totals - logdecay)
    inverse = jnp.exp(-totals)
    probed = exclusive * unit_keys
    key_in = key_heads * inverse
    removal_in = removal * inverse
    places = lax.iota(jnp.int32, sub_len)
    strict = (places[:, None] > places[None, :]).astype(jnp.float32)
    system = batch_dot(probed, flipped(removal_in)) * strict + jnp.eye(sub_len, dtype=jnp.float32)
    right_side = batch_dot(probed, flipped(carried)) + batch_dot(
        batch_dot(probed, flipped(key_in)) * strict, value_heads
    )
    solved = jax.scipy.linalg.solve_triangular(system, right_side, lower=True, unit_diagonal=True)
    final_row = inclusive[..., -1:, :]
    ending = (
        carried * final_row
        + batch_dot(flipped(value_heads), key_in * final_row)
        - batch_dot(flipped(solved), removal_in * final_row)
    )
    if not reading:
        return (ending, jnp.zeros((), jnp.float32))
    weighted = inclusive * query_heads
    upto_mask = (places[:, None] >= places[None, :]).astype(jnp.float32)
    outputs = (
        batch_dot(weighted, flipped(carried))
        + batch_dot(batch_dot(weighted, flipped(key_in)) * upto_mask, value_heads)
        - batch_dot(batch_dot(weighted, flipped(removal_in)) * upto_mask, solved)
    )
    return (ending, outputs)


def run_chain(carried, inputs, reading):
    length = inputs[0].shape[-2]
    sub_len = math.gcd(64, length)

    def to_blocks(tensor):
        leading = tensor.shape[:-2]
        shaped = tensor.reshape(leading + (length // sub_len, sub_len, tensor.shape[-1]))
        return jnp.moveaxis(shaped, -3, 0)

    def advance(state_now, pieces):
        return sub_block(state_now, pieces, reading)

    ending, outputs = lax.scan(advance, carried, tuple((to_blocks(tensor) for tensor in inputs)))
    if reading:
        outputs = jnp.moveaxis(outputs, 0, -3)
        outputs = outputs.reshape(outputs.shape[:-3] + (length, outputs.shape[-1]))
    return (ending, outputs)


def shards(
    hidden_items,
    sample_cond,
    prompt_items,
    prompt_cond,
    adjust_shifting,
    adjust_stretch,
    skip_valve,
    receiver_matrix,
    address_matrix,
    payload_matrix,
    joint_lower_projector,
    fading_raise_matrix,
    step_raise_matrix,
    feature_fading,
    spike_logfade,
    group_standard_factor,
    emit_matrix,
):
    width = hidden_items.shape[1]
    span_rows = adjust_shifting.shape[0]
    conditions = jnp.stack([sample_cond, prompt_cond])
    activated = jax.nn.silu(conditions.astype(jnp.float32)).astype(jnp.bfloat16)
    own_cols = lax.dynamic_slice_in_dim(activated, lax.axis_index("sp") * span_rows, span_rows, 1)
    part_shift = product(own_cols, adjust_shifting)
    part_scale = product(own_cols, adjust_stretch)
    part_gate = product(own_cols[:1], skip_valve)
    summed = packed_total((part_shift, part_scale, part_gate), "sp")
    shifts, scales, gates = in_one_piece((summed[0], summed[1], summed[2]), "tp", 1, 0)
    out_weight, down_weight = rows_first((emit_matrix, joint_lower_projector), "sp", (1, 0))
    u_rows = modulate(hidden_items, shifts[0], scales[0])
    low_own = stored(product(u_rows, down_weight))
    joined = jnp.concatenate([u_rows, low_own], axis=1)
    portion = lax.all_gather(joined, "tp", axis=0, tiled=True)
    features = portion[:, :width]
    gathered = jnp.concatenate(
        [
            stored(product(features, receiver_matrix)),
            stored(product(features, address_matrix)),
            stored(product(features, payload_matrix)),
            portion[:, width:],
        ],
        axis=1,
    )
    head_cols = receiver_matrix.shape[1]
    head_count = head_cols // ATTEND_WIDTH
    ctx_mod = modulate(prompt_items, shifts[1], scales[1])
    ctx_keys, ctx_values, ctx_low = in_one_piece(
        (
            stored(product(ctx_mod, address_matrix)),
            stored(product(ctx_mod, payload_matrix)),
            stored(product(ctx_mod, down_weight)),
        ),
        "sp",
        0,
        1,
    )
    ctx_inputs = chain_inputs(
        ctx_keys,
        ctx_values,
        ctx_low,
        ctx_keys,
        fading_raise_matrix,
        step_raise_matrix,
        feature_fading,
        0.0,
    )
    zeroed = jnp.zeros((2, head_count, ATTEND_WIDTH, ATTEND_WIDTH), jnp.float32)
    ctx_state, _ = run_chain(zeroed, ctx_inputs, False)
    surplus_entries = jnp.repeat(spike_logfade, ATTEND_WIDTH, axis=1)
    lat_inputs = chain_inputs(
        gathered[:, head_cols : 2 * head_cols],
        gathered[:, 2 * head_cols : 3 * head_cols],
        gathered[:, 3 * head_cols :],
        gathered[:, :head_cols],
        fading_raise_matrix,
        step_raise_matrix,
        feature_fading,
        surplus_entries,
    )
    identity_maps = jnp.broadcast_to(
        jnp.eye(ATTEND_WIDTH, dtype=jnp.float32), (2, head_count, ATTEND_WIDTH, ATTEND_WIDTH)
    )
    augmented = jnp.concatenate([jnp.zeros_like(identity_maps), identity_maps], axis=2)
    padded_values = jnp.concatenate([lat_inputs[2], jnp.zeros_like(lat_inputs[2])], axis=3)
    ending, _ = run_chain(augmented, lat_inputs[:2] + (padded_values,) + lat_inputs[3:], False)
    offsets = ending[:, :, :ATTEND_WIDTH]
    factors = ending[:, :, ATTEND_WIDTH:]

    def compose(early, later):
        return (batch_dot(early[0], later[0]), batch_dot(early[1], later[0]) + later[1])

    unit_map = (identity_maps[0], jnp.zeros_like(identity_maps[0]))
    ahead = entering((factors[0], offsets[0]), "sp", compose, unit_map)
    behind = entering_2((factors[1], offsets[1]), "sp", compose, unit_map)
    starting = jnp.stack(
        [
            batch_dot(ctx_state[0], ahead[0]) + ahead[1],
            batch_dot(ctx_state[1], behind[0]) + behind[1],
        ]
    )
    _, outputs = run_chain(starting, lat_inputs, True)
    combined = outputs[0] + jnp.flip(outputs[1], axis=1)
    centre = jnp.mean(combined, -1, keepdims=True)
    spread = jnp.mean(jnp.square(combined - centre), -1, keepdims=True)
    gains = group_standard_factor.reshape(head_count, 1, ATTEND_WIDTH)
    normed = (combined - centre) * lax.rsqrt(spread + EPS_HEAD) * gains
    row_total = combined.shape[1]
    normed = jnp.transpose(normed, (1, 0, 2)).reshape(row_total, head_cols).astype(jnp.bfloat16)
    mixed_sum = sent_and_summed(product(normed, out_weight).astype(jnp.bfloat16), "tp", 0)
    return (hidden_items.astype(jnp.float32) + gates[0] * mixed_sum).astype(jnp.bfloat16)


def solution(mesh):
    placed = (
        P(("grp", "sp", "tp"), None),
        P("grp"),
        P(("grp", "sp"), None),
        P(),
        P("sp", "tp"),
        P("sp", "tp"),
        P("sp", "tp"),
        P(None, "tp"),
        P(None, "tp"),
        P(None, "tp"),
        P("sp", None),
        P(None, "tp"),
        P(None, "tp"),
        P("tp"),
        P(("grp", "sp"), "tp"),
        P("tp"),
        P("tp", "sp"),
    )
    return jax.shard_map(
        shards, mesh=mesh, in_specs=placed, out_specs=P(("grp", "sp", "tp"), None), check_vma=False
    )
```

profile of v0, /device:TPU:65, one launch (start us, length us, event | category | flops | bytes accessed | tf_op | source)
XLA Modules:
  0.0 458.1 jit_solution(16582487184394105169)
XLA Ops:
  8.2 1.0 fusion.132
  9.2 1.1 convolution_bitcast_fusion.3
  10.4 1.1 convolution_bitcast_fusion.4
  12.1 44.2 %all-to-all-start = ((f32[16,1,1280]{2,1,0:T(1,128)}), f32[16,1,1280]{2,1,0:T(1,128)S(1)}, u32[]{:S(2)}, u32[]{:S(2)}) async-start(f32[16,1,1280]{2,1,0:T(1,128)} %broadcast_in_dim.39), calls=%async_computation | async-start | bytes 163840 | tf_op jit(solution)/shard_map/all_to_all | solution.py:16
  56.4 1.5 pad_maximum_fusion.2
  60.3 7.6 %all-to-all-done = f32[16,1,1280]{2,1,0:T(1,128)S(1)} async-done(((f32[16,1,1280]{2,1,0:T(1,128)}), f32[16,1,1280]{2,1,0:T(1,128)S(1)}, u32[]{:S(2)}, u32[]{:S(2)}) %all-to-all-start) | async-done | bytes 81952 | tf_op jit(solution)/shard_map/all_to_all | solution.py:16
  68.0 20.4 %all_gather.18 = f32[5,4096]{1,0:T(8,128)S(1)} all-gather(f32[5,256]{1,0:T(8,128)S(1)} %pad_maximum_fusion.7), channel_id=1, replica_groups=mesh['grp'=2,'sp'=16,'tp'=16] {'tp'}, dimensions={1}, use_global_device_ids=true | all-gather | bytes 87040 | tf_op jit(solution)/shard_map/all_gather | solution.py:40
  89.3 38.7 %all-gather.4.cloned.1.call-done = bf16[4096,192]{0,1:T(8,128)(2,1)} async-done(((bf16[256,192]{0,1:T(8,128)(2,1)}), bf16[4096,192]{0,1:T(8,128)(2,1)}) %all-gather.4.cloned.1.call-update) | async-done | bytes 1572880 | tf_op jit(solution)/shard_map/all_gather | solution.py:46
  128.0 1.3 convolution_convert_fusion.5
  129.3 21.7 %all_gather.20 = bf16[128,320]{1,0:T(8,128)(2,1)S(1)} all-gather(bf16[8,320]{1,0:T(8,128)(2,1)S(1)} %pad_maximum_fusion.8), channel_id=1, replica_groups=mesh['grp'=2,'sp'=16,'tp'=16] {'sp'}, dimensions={0}, use_global_device_ids=true | all-gather | bytes 87040 | tf_op jit(solution)/shard_map/all_gather | solution.py:40
  152.9 1.3 convolution_convert_fusion.4
  155.7 1.0 maximum_bitcast_fusion
  157.0 46.8 %while.51 = (s32[]{:T(128)}, f32[2,2,64,64]{3,2,1,0:T(8,128)S(1)}, f32[2,2,2,64,64]{3,0,4,2,1:T(2,128)}, f32[2,2,2,64,64]{3,0,4,2,1:T(2,128)S(1)}, f32[2,2,2,64,...) while((s32[]{:T(128)}, f32[2,2,64,64]{3,2,1,0:T(8,128)S(1)}, ...), condition=%wide.region_6.8_spmd.clone, body=%wide.region_4.7_spmd.clone.sunk | while | flops 26669124 | bytes 3338888 | solution.py:265
  157.3 1.1 constant_dynamic-slice_fusion.16
  160.1 19.7 %custom-call.18 = f32[2,2,1,64,64]{3,4,2,1,0:T(8,128)S(1)} custom-call(f32[2,2,1,64,64]{4,3,2,1,0:T(8,128)S(1)} %fusion.288), custom_call_target="InvertDiagBlocksLowerTriangular" | custom-call | tf_op jit(solution)/shard_map/while/body/eval_jaxpr/jit(_solve_triangular)/vmap(vmap())/triangular_solve | solution.py:234
  180.7 1.1 constant_dynamic-slice_fusion.16
  183.5 19.7 %custom-call.18 = f32[2,2,1,64,64]{3,4,2,1,0:T(8,128)S(1)} custom-call(f32[2,2,1,64,64]{4,3,2,1,0:T(8,128)S(1)} %fusion.288), custom_call_target="InvertDiagBlocksLowerTriangular" | custom-call | tf_op jit(solution)/shard_map/while/body/eval_jaxpr/jit(_solve_triangular)/vmap(vmap())/triangular_solve | solution.py:234
  203.8 10.1 %all-gather.6.cloned.1.call-done = bf16[128,4160]{1,0:T(8,128)(2,1)} async-done(((bf16[8,4160]{1,0:T(8,128)(2,1)}), bf16[128,4160]{1,0:T(8,128)(2,1)}) %all-gather.6.cloned.1.call-update) | async-done | bytes 1064976 | tf_op jit(solution)/shard_map/all_gather | solution.py:305
  213.9 1.0 fusion.83
  215.2 1.7 convolution_convert_fusion.2
  217.2 1.0 fusion.78
  220.3 1.6 convolution_convert_fusion.3
  224.1 42.9 %while.49 = (s32[]{:T(128)}, f32[2,2,128,64]{2,3,1,0:T(8,128)S(1)}, f32[2,2,2,64,64]{4,3,2,1,0:T(8,128)S(1)}, bf16[2,2,2,64,128]{4,3,0,2,1:T(8,128)(2,1)S(1)}, f...) while((s32[]{:T(128)}, f32[2,2,128,64]{2,3,1,0:T(8,128)S(1)}, ...), condition=%wide.region_12.14_spmd, body=%wide.region_10.13_spmd.sunk | while | flops 47673408 | bytes 4268149 | solution.py:265
  225.3 19.7 %custom-call.16 = f32[2,2,1,64,64]{3,4,2,1,0:T(8,128)S(1)} custom-call(f32[2,2,1,64,64]{4,3,2,1,0:T(8,128)S(1)} %fusion.251), custom_call_target="InvertDiagBlocksLowerTriangular" | custom-call | tf_op jit(solution)/shard_map/while/body/eval_jaxpr/jit(_solve_triangular)/vmap(vmap())/triangular_solve | solution.py:234
  246.7 19.7 %custom-call.16 = f32[2,2,1,64,64]{3,4,2,1,0:T(8,128)S(1)} custom-call(f32[2,2,1,64,64]{4,3,2,1,0:T(8,128)S(1)} %fusion.251), custom_call_target="InvertDiagBlocksLowerTriangular" | custom-call | tf_op jit(solution)/shard_map/while/body/eval_jaxpr/jit(_solve_triangular)/vmap(vmap())/triangular_solve | solution.py:234
  267.4 0.8 broadcast_in_dim.44
  268.3 12.5 %all-to-all-start.1 = ((bf16[16,256,64]{1,2,0:T(8,128)(2,1)}), bf16[16,256,64]{1,2,0:T(8,128)(2,1)S(1)}, u32[]{:S(2)}, u32[]{:S(2)}) async-start(bf16[16,256,64]{1,2,0:T(8,128)(2,1)} %broadcast_in_dim.44), calls=%async_computation.1 | async-start | bytes 1048576 | tf_op jit(solution)/shard_map/all_to_all | solution.py:16
  281.1 45.0 %all-gather = bf16[4096,64]{0,1:T(8,128)(2,1)S(1)} all-gather(bf16[256,64]{0,1:T(8,128)(2,1)S(1)} %pad_maximum_fusion.4), channel_id=2, replica_groups=mesh['grp'=2,'sp'=16,'tp'=16] {'sp'}, dimensions={0}, use_global_device_ids=true | all-gather | bytes 557056 | tf_op jit(solution)/shard_map/all_gather | solution.py:62
  326.4 1.1 reshape_reshape.8
  327.5 1.1 reshape_reshape.9
  328.6 18.0 %while.52 = (s32[]{:T(128)}, bf16[2,64,64]{1,2,0:T(8,128)(2,1)S(1)}, f32[2,64,64]{1,2,0:T(8,128)S(1)}, s32[]{:T(128)}, bf16[16,2,64,64]{2,1,3,0:T(2,128)(2,1)}, ...) while((s32[]{:T(128)}, bf16[2,64,64]{1,2,0:T(8,128)(2,1)S(1)}, ...), condition=%wide.region_14.16_spmd.clone, body=%wide.region_13.15_spmd.clone.sunk | while | flops 2146308 | bytes 311414 | solution.py:90
  328.7 0.8 constant_dynamic-slice_fusion.18
  329.8 0.8 constant_dynamic-slice_fusion.18
  330.9 0.8 constant_dynamic-slice_fusion.18
  332.0 0.8 constant_dynamic-slice_fusion.18
  333.2 0.8 constant_dynamic-slice_fusion.18
  335.4 0.8 constant_dynamic-slice_fusion.18
  346.9 2.0 convolution_convert_fusion.1
  350.2 1.1 maximum_bitcast_fusion.9
  351.3 1.0 fusion.140
  352.3 1.4 copy.217
  358.2 49.5 %while.50 = (s32[]{:T(128)}, f32[2,2,64,64]{3,2,1,0:T(8,128)S(1)}, f32[2,2,2,64,64]{4,3,2,1,0:T(8,128)}, f32[2,2,2,64,64]{4,3,2,1,0:T(8,128)S(1)}, f32[2,2,2,64,...) while((s32[]{:T(128)}, f32[2,2,64,64]{3,2,1,0:T(8,128)S(1)}, ...), condition=%wide.region_17.19_spmd, body=%wide.region_15.18_spmd.sunk | while | flops 37163072 | bytes 5173957 | solution.py:265
  358.2 1.3 constant_dynamic-slice_fusion.14
  360.9 19.7 %custom-call.17 = f32[2,2,1,64,64]{3,4,2,1,0:T(8,128)S(1)} custom-call(f32[2,2,1,64,64]{4,3,2,1,0:T(8,128)S(1)} %fusion.273), custom_call_target="InvertDiagBlocksLowerTriangular" | custom-call | tf_op jit(solution)/shard_map/while/body/eval_jaxpr/jit(_solve_triangular)/vmap(vmap())/triangular_solve | solution.py:234
  383.0 1.3 constant_dynamic-slice_fusion.14
  385.7 19.7 %custom-call.17 = f32[2,2,1,64,64]{3,4,2,1,0:T(8,128)S(1)} custom-call(f32[2,2,1,64,64]{4,3,2,1,0:T(8,128)S(1)} %fusion.273), custom_call_target="InvertDiagBlocksLowerTriangular" | custom-call | tf_op jit(solution)/shard_map/while/body/eval_jaxpr/jit(_solve_triangular)/vmap(vmap())/triangular_solve | solution.py:234
  407.7 1.1 fusion.141
  410.0 39.7 %all_to_all.16 = bf16[16,8,4096]{2,1,0:T(8,128)(2,1)S(1)} all-to-all(bf16[16,8,4096]{2,1,0:T(8,128)(2,1)S(1)} %fusion.70), channel_id=1, replica_groups=mesh['grp'=2,'sp'=16,'tp'=16] {'tp'}, dimensions={0} | all-to-all | bytes 2097152 | tf_op jit(solution)/shard_map/all_to_all | solution.py:145
  (386 shorter events, 51.7 us)
Async XLA Ops:
  6.5 82.3 %copy-start = (bf16[4096,128]{1,0:T(8,128)(2,1)S(1)}, bf16[4096,128]{1,0:T(8,128)(2,1)}, u32[]{:S(2)}) copy-start(bf16[4096,128]{1,0:T(8,128)(2,1)} %param.35) | copy-start | bytes 3145732
  6.6 51.5 %copy-start.3 = (bf16[8,4096]{1,0:T(8,128)(2,1)S(1)}, bf16[8,4096]{1,0:T(8,128)(2,1)}, u32[]{:S(2)}) copy-start(bf16[8,4096]{1,0:T(8,128)(2,1)} %param.27) | copy-start | bytes 196612
  6.6 51.9 %copy-start.7 = (bf16[8,4096]{1,0:T(8,128)(2,1)S(1)}, bf16[8,4096]{1,0:T(8,128)(2,1)}, u32[]{:S(2)}) copy-start(bf16[8,4096]{1,0:T(8,128)(2,1)} %param.29) | copy-start | bytes 196612
  6.6 53.0 %copy-start.27 = (f32[128]{0:T(128)S(1)}, f32[128]{0:T(128)}, u32[]{:S(2)}) copy-start(f32[128]{0:T(128)} %param.40) | copy-start | bytes 1540
  6.6 53.0 %copy-start.28 = (f32[128]{0:T(128)S(1)}, f32[128]{0:T(128)}, u32[]{:S(2)}) copy-start(f32[128]{0:T(128)} %param.42) | copy-start | bytes 1540
  9.2 79.3 %copy-start.5 = (bf16[4096,128]{1,0:T(8,128)(2,1)S(1)}, bf16[4096,128]{1,0:T(8,128)(2,1)}, u32[]{:S(2)}) copy-start(bf16[4096,128]{1,0:T(8,128)(2,1)} %param.36) | copy-start | bytes 3145732
  12.1 55.8 %all-to-all-start = ((f32[16,1,1280]{2,1,0:T(1,128)}), f32[16,1,1280]{2,1,0:T(1,128)S(1)}, u32[]{:S(2)}, u32[]{:S(2)}) async-start(f32[16,1,1280]{2,1,0:T(1,128)} %broadcast_in_dim.39), calls=%async_computation | async-start | bytes 163840 | tf_op jit(solution)/shard_map/all_to_all | solution.py:16
  56.3 71.6 %all-gather.4.cloned.1.call-start = ((), (), s32[]{:S(2)}) async-start(), calls=%async_computation.3 | async-start | bytes 1671168 | tf_op jit(solution)/shard_map/all_gather | solution.py:46
  58.0 155.9 %all-gather.6.cloned.1.call-start = ((), (), s32[]{:S(2)}) async-start(), calls=%async_computation.4 | async-start | bytes 1148928 | tf_op jit(solution)/shard_map/all_gather | solution.py:305
  58.1 2.1 copy-start.11
  59.5 0.7 copy-start.13
  88.9 62.2 %copy-start.24 = (bf16[64,128]{1,0:T(8,128)(2,1)S(1)}, bf16[64,128]{1,0:T(8,128)(2,1)}, u32[]{:S(2)}) copy-start(bf16[64,128]{1,0:T(8,128)(2,1)} %param.38) | copy-start | bytes 49156
  129.3 22.9 %copy-start.25 = (bf16[64,128]{1,0:T(8,128)(2,1)S(1)}, bf16[64,128]{1,0:T(8,128)(2,1)}, u32[]{:S(2)}) copy-start(bf16[64,128]{1,0:T(8,128)(2,1)} %param.39) | copy-start | bytes 49156
  157.0 56.9 %copy-start.22 = (f32[128,2]{0,1:T(2,128)S(1)}, f32[128,2]{0,1:T(2,128)}, u32[]{:S(2)}) copy-start(f32[128,2]{0,1:T(2,128)} %param.41) | copy-start | bytes 3076
  215.1 2.0 copy-start.26
  218.2 2.2 copy-start.6
  222.0 1.1 copy-start.16
  222.2 0.6 copy-start.8
  222.8 0.8 copy-start.15
  268.3 83.0 %all-to-all-start.1 = ((bf16[16,256,64]{1,2,0:T(8,128)(2,1)}), bf16[16,256,64]{1,2,0:T(8,128)(2,1)S(1)}, u32[]{:S(2)}, u32[]{:S(2)}) async-start(bf16[16,256,64]{1,2,0:T(8,128)(2,1)} %broadcast_in_dim.44), calls=%async_computation.1 | async-start | bytes 1048576 | tf_op jit(solution)/shard_map/all_to_all | solution.py:16
  326.4 2.2 copy-start.14
  328.6 18.1 %copy-start.9 = (f32[2,128,64]{1,2,0:T(8,128)S(1)}, f32[2,128,64]{1,2,0:T(8,128)}, u32[]{:S(2)}) copy-start(f32[2,128,64]{1,2,0:T(8,128)} %copy-done.8) | copy-start | bytes 196612
  352.3 1.4 copy-start.21
  353.9 1.6 copy-start.2
  353.9 1.9 copy-start.12
  356.0 1.0 copy-start.10
  356.0 1.1 copy-start.19
  357.3 0.9 copy-start.20
  381.0 1.0 copy-start.17
  382.2 0.7 copy-start.18
  405.7 1.0 copy-start.17
  407.0 0.7 copy-start.18
  407.7 1.8 copy-start.23
  407.7 1.9 copy-start.1
  449.8 0.8 copy-start.4
Sparse Core Ops, SparseCore 0:
  59.2 68.7 all-gather.3
  155.0 58.8 all-gather.5
where the time goes:
time: 460 us; the launch traced here: 458 us
  other arithmetic  129 us (28%)
  blocking collectives  127 us (28%)
  starting transfers between devices  56.9 us (12%)
  waiting for transfers between devices  56.5 us (12%)
  local copies, waits for them, and re-layouts  42.8 us (9%)
  matrix products  30.6 us (7%)
  between operations  14.5 us (3%)
    another operation x18, other arithmetic, sub_block(): jax.scipy.linalg.solve_triangular(system, right_side, lower=True, unit_di...  119 us
    all_to_all x2, starting transfers between devices, copy_for_each(): lax.all_to_all(jnp.broadcast_to(shard[None], (peers, *shard.shape)), axis...  56.7 us
    all_gather x1, blocking collectives, collected_together(): both, at, found = (lax.all_gather(jnp.concatenate(lines), axis), 0, {})  45 us
    all_gather x2, blocking collectives, in_one_piece(): lax.all_gather(both, axis, axis=dim, tiled=True)  42.1 us
    all_to_all x1, blocking collectives, sent_and_summed(): tiles = lax.all_to_all(cut_along(shard, dim, peers), axis, 0, 0, tiled=True)  39.7 us
    all_gather x1, waiting for transfers between devices, rows_first(): lax.all_gather(both, axis, axis=0, tiled=True)  38.7 us
    dot_general x15, matrix products, product(): return jnp.dot(left, right, preferred_element_type=jnp.float32)  14.6 us
    dot_general x77, matrix products, batch_dot(): return jnp.matmul(left, right)  13.7 us
  transfers between devices with their start and end apart: 4, of which 3 were waited for; matrix products, arithmetic and copies ran while one was open for 17% of the time, Pallas kernels for 0%

commit v1 on v0

--- a/solution.py
+++ b/solution.py
@@ -43,7 +43,13 @@
 def rows_first(arrays, axis, dims):
     turned = [jnp.moveaxis(a, dim, 0) for a, dim in zip(arrays, dims)]
     both = jnp.concatenate([t.reshape(len(t), -1) for t in turned], axis=1)
-    result, at, gathered = (lax.all_gather(both, axis, axis=0, tiled=True), 0, [])
+    result, at, gathered = (
+        jnp.concatenate(
+            lax.all_to_all(jnp.stack([both] * lax.axis_size(axis)), axis, 0, 0), axis=0
+        ),
+        0,
+        [],
+    )
     for t, dim in zip(turned, dims):
         slab = result[:, at : at + t[0].size].reshape(-1, *t.shape[1:])
         gathered.append(jnp.moveaxis(slab, 0, dim))

time: 460 us -> 476 us (1.035)
  local copies, waits for them, and re-layouts: 42.8 us -> 52.5 us
    all_to_all x0 -> x1, waiting for transfers between devices: none -> 44.5 us  [rows_first(): lax.all_to_all(jnp.stack([both] * lax.axis_size(axis)), axis, 0, 0)]
    all_gather x1 -> x0, waiting for transfers between devices: 38.7 us -> none  [rows_first(): lax.all_gather(both, axis, axis=0, tiled=True)]
    all_gather x1, waiting for transfers between devices: 10.1 us -> 0.46 us  [shards(): portion = lax.all_gather(joined, 'tp', axis=0, tiled=True)]
    another operation x22, local copies, waits for them, and re-layouts: 2.9 us -> 8.36 us  [both_ways(): return jnp.stack([tensor, jnp.flip(tensor, axis=1)])]
where the time goes in v1:
time: 476 us; the launch traced here: 473 us
  other arithmetic  128 us (27%)
  blocking collectives  128 us (27%)
  starting transfers between devices  61.6 us (13%)
  waiting for transfers between devices  55.7 us (12%)
  local copies, waits for them, and re-layouts  52.5 us (11%)
  matrix products  31 us (7%)
  between operations  14.5 us (3%)
    another operation x18, other arithmetic, sub_block(): jax.scipy.linalg.solve_triangular(system, right_side, lower=True, unit_di...  119 us
    all_to_all x2, starting transfers between devices, copy_for_each(): lax.all_to_all(jnp.broadcast_to(shard[None], (peers, *shard.shape)), axis...  56.9 us
    all_gather x1, blocking collectives, collected_together(): both, at, found = (lax.all_gather(jnp.concatenate(lines), axis), 0, {})  44.9 us
    all_to_all x1, waiting for transfers between devices, rows_first(): lax.all_to_all(jnp.stack([both] * lax.axis_size(axis)), axis, 0, 0)  44.5 us
    all_gather x2, blocking collectives, in_one_piece(): lax.all_gather(both, axis, axis=dim, tiled=True)  43.4 us
    all_to_all x1, blocking collectives, sent_and_summed(): tiles = lax.all_to_all(cut_along(shard, dim, peers), axis, 0, 0, tiled=True)  40.1 us
    dot_general x77, matrix products, batch_dot(): return jnp.matmul(left, right)  15 us
    dot_general x15, matrix products, product(): return jnp.dot(left, right, preferred_element_type=jnp.float32)  13.6 us
  transfers between devices with their start and end apart: 4, of which 3 were waited for; matrix products, arithmetic and copies ran while one was open for 17% of the time, Pallas kernels for 0%

profile of v1, /device:TPU:65, one launch (start us, length us, event | category | flops | bytes accessed | tf_op | source)
XLA Modules:
  0.0 473.1 jit_solution(10789169859672827436)
XLA Ops:
  8.1 1.0 fusion.132
  9.2 1.1 convolution_bitcast_fusion.3
  10.2 1.1 convolution_bitcast_fusion.4
  12.0 44.2 %all-to-all-start = ((f32[16,1,1280]{2,1,0:T(1,128)}), f32[16,1,1280]{2,1,0:T(1,128)S(1)}, u32[]{:S(2)}, u32[]{:S(2)}) async-start(f32[16,1,1280]{2,1,0:T(1,128)} %broadcast_in_dim.39), calls=%async_computation | async-start | bytes 163840 | tf_op jit(solution)/shard_map/all_to_all | solution.py:16
  57.1 10.7 %all-to-all-done = f32[16,1,1280]{2,1,0:T(1,128)S(1)} async-done(((f32[16,1,1280]{2,1,0:T(1,128)}), f32[16,1,1280]{2,1,0:T(1,128)S(1)}, u32[]{:S(2)}, u32[]{:S(2)}) %all-to-all-start) | async-done | bytes 81952 | tf_op jit(solution)/shard_map/all_to_all | solution.py:16
  67.8 1.4 stack.145
  69.2 4.6 all-to-all-start.1
  76.3 20.1 %all_gather.15 = f32[5,4096]{1,0:T(8,128)S(1)} all-gather(f32[5,256]{1,0:T(8,128)S(1)} %pad_maximum_fusion.7), channel_id=1, replica_groups=mesh['grp'=2,'sp'=16,'tp'=16] {'tp'}, dimensions={1}, use_global_device_ids=true | all-gather | bytes 87040 | tf_op jit(solution)/shard_map/all_gather | solution.py:40
  96.4 1.5 convolution_convert_fusion.6
  98.4 44.5 %all-to-all-done.1 = bf16[16,256,192]{1,2,0:T(8,128)(2,1)S(1)} async-done(((bf16[16,256,192]{1,2,0:T(8,128)(2,1)}), bf16[16,256,192]{1,2,0:T(8,128)(2,1)S(1)}, u32[]{:S(2)}, u32[]{:S(2)}) %all-to-all-start.1) | async-done | bytes 1572896 | tf_op jit(solution)/shard_map/all_to_all | solution.py:48
  142.9 1.2 copy-done.3
  144.1 1.6 copy.312
  146.0 23.3 %all_gather.16 = bf16[128,320]{1,0:T(8,128)(2,1)S(1)} all-gather(bf16[8,320]{1,0:T(8,128)(2,1)S(1)} %pad_maximum_fusion.8), channel_id=1, replica_groups=mesh['grp'=2,'sp'=16,'tp'=16] {'sp'}, dimensions={0}, use_global_device_ids=true | all-gather | bytes 87040 | tf_op jit(solution)/shard_map/all_gather | solution.py:40
  176.7 1.0 stack.147
  177.6 1.0 stack.150
  178.6 1.0 stack.153
  179.6 1.0 stack.156
  180.5 1.0 stack.159
  181.7 1.0 maximum_bitcast_fusion
  183.0 46.8 %while.51 = (s32[]{:T(128)}, f32[2,2,64,64]{3,2,1,0:T(8,128)S(1)}, f32[2,2,2,64,64]{3,0,4,2,1:T(2,128)}, f32[2,2,2,64,64]{3,0,4,2,1:T(2,128)S(1)}, f32[2,2,2,64,...) while((s32[]{:T(128)}, f32[2,2,64,64]{3,2,1,0:T(8,128)S(1)}, ...), condition=%wide.region_6.8_spmd.clone, body=%wide.region_4.7_spmd.clone.sunk | while | flops 26669124 | bytes 3338888 | solution.py:271
  183.3 1.1 constant_dynamic-slice_fusion.16
  186.1 19.7 %custom-call.18 = f32[2,2,1,64,64]{3,4,2,1,0:T(8,128)S(1)} custom-call(f32[2,2,1,64,64]{4,3,2,1,0:T(8,128)S(1)} %fusion.288), custom_call_target="InvertDiagBlocksLowerTriangular" | custom-call | tf_op jit(solution)/shard_map/while/body/eval_jaxpr/jit(_solve_triangular)/vmap(vmap())/triangular_solve | solution.py:240
  206.6 1.1 constant_dynamic-slice_fusion.16
  209.5 19.7 %custom-call.18 = f32[2,2,1,64,64]{3,4,2,1,0:T(8,128)S(1)} custom-call(f32[2,2,1,64,64]{4,3,2,1,0:T(8,128)S(1)} %fusion.288), custom_call_target="InvertDiagBlocksLowerTriangular" | custom-call | tf_op jit(solution)/shard_map/while/body/eval_jaxpr/jit(_solve_triangular)/vmap(vmap())/triangular_solve | solution.py:240
  230.2 1.0 fusion.83
  231.4 1.6 convolution_convert_fusion.2
  233.5 1.0 fusion.78
  236.6 1.6 convolution_convert_fusion.3
  240.3 42.9 %while.49 = (s32[]{:T(128)}, f32[2,2,128,64]{2,3,1,0:T(8,128)S(1)}, f32[2,2,2,64,64]{4,3,2,1,0:T(8,128)S(1)}, bf16[2,2,2,64,128]{4,3,0,2,1:T(8,128)(2,1)S(1)}, f...) while((s32[]{:T(128)}, f32[2,2,128,64]{2,3,1,0:T(8,128)S(1)}, ...), condition=%wide.region_12.14_spmd, body=%wide.region_10.13_spmd.sunk | while | flops 47673408 | bytes 4268149 | solution.py:271
  241.4 19.7 %custom-call.16 = f32[2,2,1,64,64]{3,4,2,1,0:T(8,128)S(1)} custom-call(f32[2,2,1,64,64]{4,3,2,1,0:T(8,128)S(1)} %fusion.251), custom_call_target="InvertDiagBlocksLowerTriangular" | custom-call | tf_op jit(solution)/shard_map/while/body/eval_jaxpr/jit(_solve_triangular)/vmap(vmap())/triangular_solve | solution.py:240
  262.9 19.7 %custom-call.16 = f32[2,2,1,64,64]{3,4,2,1,0:T(8,128)S(1)} custom-call(f32[2,2,1,64,64]{4,3,2,1,0:T(8,128)S(1)} %fusion.251), custom_call_target="InvertDiagBlocksLowerTriangular" | custom-call | tf_op jit(solution)/shard_map/while/body/eval_jaxpr/jit(_solve_triangular)/vmap(vmap())/triangular_solve | solution.py:240
  284.5 12.7 %all-to-all-start.2 = ((bf16[16,256,64]{1,2,0:T(8,128)(2,1)}), bf16[16,256,64]{1,2,0:T(8,128)(2,1)S(1)}, u32[]{:S(2)}, u32[]{:S(2)}) async-start(bf16[16,256,64]{1,2,0:T(8,128)(2,1)} %broadcast_in_dim.44), calls=%async_computation.2 | async-start | bytes 1048576 | tf_op jit(solution)/shard_map/all_to_all | solution.py:16
  297.5 44.9 %all-gather = bf16[4096,64]{0,1:T(8,128)(2,1)S(1)} all-gather(bf16[256,64]{0,1:T(8,128)(2,1)S(1)} %pad_maximum_fusion.4), channel_id=2, replica_groups=mesh['grp'=2,'sp'=16,'tp'=16] {'sp'}, dimensions={0}, use_global_device_ids=true | all-gather | bytes 557056 | tf_op jit(solution)/shard_map/all_gather | solution.py:68
  342.7 1.1 reshape_reshape.8
  343.8 1.0 reshape_reshape.9
  344.9 18.0 %while.52 = (s32[]{:T(128)}, bf16[2,64,64]{1,2,0:T(8,128)(2,1)S(1)}, f32[2,64,64]{1,2,0:T(8,128)S(1)}, s32[]{:T(128)}, bf16[16,2,64,64]{2,1,3,0:T(2,128)(2,1)}, ...) while((s32[]{:T(128)}, bf16[2,64,64]{1,2,0:T(8,128)(2,1)S(1)}, ...), condition=%wide.region_14.16_spmd.clone, body=%wide.region_13.15_spmd.clone.sunk | while | flops 2146308 | bytes 311414 | solution.py:96
  363.2 2.0 convolution_convert_fusion.1
  366.5 1.1 maximum_bitcast_fusion.9
  367.6 1.0 fusion.140
  368.6 1.4 copy.272
  374.5 48.5 %while.50 = (s32[]{:T(128)}, f32[2,2,64,64]{3,2,1,0:T(8,128)S(1)}, f32[2,2,2,64,64]{4,3,2,1,0:T(8,128)}, f32[2,2,2,64,64]{4,3,2,1,0:T(8,128)S(1)}, f32[2,2,2,64,...) while((s32[]{:T(128)}, f32[2,2,64,64]{3,2,1,0:T(8,128)S(1)}, ...), condition=%wide.region_17.19_spmd, body=%wide.region_15.18_spmd.sunk | while | flops 37163072 | bytes 3814029 | solution.py:271
  374.5 1.3 constant_dynamic-slice_fusion.14
  377.2 19.7 %custom-call.17 = f32[2,2,1,64,64]{3,4,2,1,0:T(8,128)S(1)} custom-call(f32[2,2,1,64,64]{4,3,2,1,0:T(8,128)S(1)} %fusion.273), custom_call_target="InvertDiagBlocksLowerTriangular" | custom-call | tf_op jit(solution)/shard_map/while/body/eval_jaxpr/jit(_solve_triangular)/vmap(vmap())/triangular_solve | solution.py:240
  397.8 1.0 fusion.277
  398.7 1.3 constant_dynamic-slice_fusion.14
  401.4 19.7 %custom-call.17 = f32[2,2,1,64,64]{3,4,2,1,0:T(8,128)S(1)} custom-call(f32[2,2,1,64,64]{4,3,2,1,0:T(8,128)S(1)} %fusion.273), custom_call_target="InvertDiagBlocksLowerTriangular" | custom-call | tf_op jit(solution)/shard_map/while/body/eval_jaxpr/jit(_solve_triangular)/vmap(vmap())/triangular_solve | solution.py:240
  423.0 1.1 fusion.141
  425.3 40.1 %all_to_all.21 = bf16[16,8,4096]{2,1,0:T(8,128)(2,1)S(1)} all-to-all(bf16[16,8,4096]{2,1,0:T(8,128)(2,1)S(1)} %fusion.70), channel_id=1, replica_groups=mesh['grp'=2,'sp'=16,'tp'=16] {'tp'}, dimensions={0} | all-to-all | bytes 2097152 | tf_op jit(solution)/shard_map/all_to_all | solution.py:151
  (389 shorter events, 60.0 us)
Async XLA Ops:
  6.5 91.4 %copy-start = (bf16[4096,128]{1,0:T(8,128)(2,1)S(1)}, bf16[4096,128]{1,0:T(8,128)(2,1)}, u32[]{:S(2)}) copy-start(bf16[4096,128]{1,0:T(8,128)(2,1)} %param.35) | copy-start | bytes 3145732
  12.0 55.8 %all-to-all-start = ((f32[16,1,1280]{2,1,0:T(1,128)}), f32[16,1,1280]{2,1,0:T(1,128)S(1)}, u32[]{:S(2)}, u32[]{:S(2)}) async-start(f32[16,1,1280]{2,1,0:T(1,128)} %broadcast_in_dim.39), calls=%async_computation | async-start | bytes 163840 | tf_op jit(solution)/shard_map/all_to_all | solution.py:16
  69.2 4.8 %copy-start.28 = (f32[128]{0:T(128)S(1)}, f32[128]{0:T(128)}, u32[]{:S(2)}) copy-start(f32[128]{0:T(128)} %param.40) | copy-start | bytes 1540
  69.2 4.9 %copy-start.29 = (f32[128]{0:T(128)S(1)}, f32[128]{0:T(128)}, u32[]{:S(2)}) copy-start(f32[128]{0:T(128)} %param.42) | copy-start | bytes 1540
  69.2 6.2 %copy-start.5 = (bf16[8,4096]{1,0:T(8,128)(2,1)S(1)}, bf16[8,4096]{1,0:T(8,128)(2,1)}, u32[]{:S(2)}) copy-start(bf16[8,4096]{1,0:T(8,128)(2,1)} %param.27) | copy-start | bytes 196612
  69.2 6.4 %copy-start.8 = (bf16[8,4096]{1,0:T(8,128)(2,1)S(1)}, bf16[8,4096]{1,0:T(8,128)(2,1)}, u32[]{:S(2)}) copy-start(bf16[8,4096]{1,0:T(8,128)(2,1)} %param.29) | copy-start | bytes 196612
  69.2 73.7 %all-to-all-start.1 = ((bf16[16,256,192]{1,2,0:T(8,128)(2,1)}), bf16[16,256,192]{1,2,0:T(8,128)(2,1)S(1)}, u32[]{:S(2)}, u32[]{:S(2)}) async-start(bf16[16,256,192]{1,2,0:T(8,128)(2,1)} %stack.145), calls=%async_computation.1 | async-start | bytes 3145728 | tf_op jit(solution)/shard_map/all_to_all | solution.py:48
  73.8 156.4 %all-gather.3.cloned.1.call-start = ((), (), s32[]{:S(2)}) async-start(), calls=%async_computation.4 | async-start | bytes 1148928 | tf_op jit(solution)/shard_map/all_gather | solution.py:311
  73.9 0.8 copy-start.14
  74.0 0.7 copy-start.16
  74.0 95.3 %copy-start.30 = (f32[128]{0:T(128)}, f32[128]{0:T(128)S(1)}, u32[]{:S(2)}) copy-start(f32[128]{0:T(128)S(1)} %neg.30) | copy-start | bytes 1540
  142.9 1.2 copy-start.3
  144.1 25.3 %copy-start.25 = (bf16[64,128]{1,0:T(8,128)(2,1)S(1)}, bf16[64,128]{1,0:T(8,128)(2,1)}, u32[]{:S(2)}) copy-start(bf16[64,128]{1,0:T(8,128)(2,1)} %param.38) | copy-start | bytes 49156
  145.7 30.0 %copy-start.1 = (bf16[16,24,8,256]{3,2,0,1:T(8,128)(2,1)}, bf16[16,24,8,256]{3,2,0,1:T(8,128)(2,1)S(1)}, u32[]{:S(2)}) copy-start(bf16[16,24,8,256]{3,2,0,1:T(8,128)(2,1)S(1)} %copy.312) | copy-start | bytes 4718596
  145.7 27.3 %copy-start.26 = (bf16[64,128]{1,0:T(8,128)(2,1)S(1)}, bf16[64,128]{1,0:T(8,128)(2,1)}, u32[]{:S(2)}) copy-start(bf16[64,128]{1,0:T(8,128)(2,1)} %param.39) | copy-start | bytes 49156
  175.7 7.0 %copy-start.12 = (f32[1,2,2,64,64]{3,2,4,1,0:T(2,128)S(1)}, f32[1,2,2,64,64]{3,2,4,1,0:T(2,128)}, u32[]{:S(2)}) copy-start(f32[1,2,2,64,64]{3,2,4,1,0:T(2,128)} %stack.152) | copy-start | bytes 196612
  175.9 6.7 %copy-start.13 = (f32[1,2,2,64,64]{3,2,4,1,0:T(2,128)S(1)}, f32[1,2,2,64,64]{3,2,4,1,0:T(2,128)}, u32[]{:S(2)}) copy-start(f32[1,2,2,64,64]{3,2,4,1,0:T(2,128)} %stack.155) | copy-start | bytes 196612
  182.9 47.3 %copy-start.23 = (f32[128,2]{0,1:T(2,128)S(1)}, f32[128,2]{0,1:T(2,128)}, u32[]{:S(2)}) copy-start(f32[128,2]{0,1:T(2,128)} %param.41) | copy-start | bytes 3076
  183.0 47.3 %copy-start.31 = (f32[128]{0:T(128)S(1)}, f32[128]{0:T(128)}, u32[]{:S(2)}) copy-start(f32[128]{0:T(128)} %copy-done.30) | copy-start | bytes 1540
  231.2 2.3 copy-start.27
  233.1 3.5 copy-start.7
  238.3 1.1 copy-start.19
  238.5 0.6 copy-start.9
  238.5 1.4 copy-start.18
  284.5 83.1 %all-to-all-start.2 = ((bf16[16,256,64]{1,2,0:T(8,128)(2,1)}), bf16[16,256,64]{1,2,0:T(8,128)(2,1)S(1)}, u32[]{:S(2)}, u32[]{:S(2)}) async-start(bf16[16,256,64]{1,2,0:T(8,128)(2,1)} %broadcast_in_dim.44), calls=%async_computation.2 | async-start | bytes 1048576 | tf_op jit(solution)/shard_map/all_to_all | solution.py:16
  342.6 2.3 copy-start.17
  344.9 18.1 %copy-start.10 = (f32[2,128,64]{1,2,0:T(8,128)S(1)}, f32[2,128,64]{1,2,0:T(8,128)}, u32[]{:S(2)}) copy-start(f32[2,128,64]{1,2,0:T(8,128)} %copy-done.9) | copy-start | bytes 196612
  367.6 2.4 copy-start.22
  370.1 1.7 copy-start.4
  370.2 1.9 copy-start.15
  372.3 1.0 copy-start.11
  372.3 1.1 copy-start.20
  373.4 1.1 copy-start.21
  423.0 1.8 copy-start.24
  423.0 1.9 copy-start.2
  425.3 40.3 %copy-start.6 = (bf16[8,4096]{1,0:T(8,128)(2,1)S(1)}, bf16[8,4096]{1,0:T(8,128)(2,1)}, u32[]{:S(2)}) copy-start(bf16[8,4096]{1,0:T(8,128)(2,1)} %param.27) | copy-start | bytes 196612
Sparse Core Ops, SparseCore 0:
  176.8 53.3 all-gather.2
